TPU v7x, 32 devices: a whole 2x2x4 slice. The times are simulated.
32 devices in a mesh: grp: 2 (over y), sp: 4 (over z), tp: 4 (over x, core).
Axes of the slice: x: 2, y: 2, z: 4, core: 2. Of those that a mesh axis runs over, the one named last changes fastest.
Arguments:
- hidden_in: bfloat16 [2048, 2048], P(('grp', 'sp')), parts along dimension 0, may hold values from -6 to 6
- query_latent_rows: bfloat16 [2048, 768], P(('grp', 'sp')), parts along dimension 0, may hold values from -6 to 6
- key_value_latent: bfloat16 [2048, 512], P(('grp', 'sp')), parts along dimension 0, may hold values from -6 to 6
- rotary_key: bfloat16 [2048, 32], P(('grp', 'sp')), parts along dimension 0, may hold values from -64 to 64
- query_norm_gain: float32 [768], replicated, may hold values from 0.1 to 1.9
- key_value_gain: float32 [512], replicated, may hold values from 0.1 to 1.9
- query_up_weight: bfloat16 [768, 1536], P(None, 'tp'), may hold values from -0.625 to 0.625
- key_value_up_weight: bfloat16 [512, 2048], P(None, 'tp'), may hold values from -0.25 to 0.25
- out_proj: bfloat16 [1024, 2048], P('tp'), may hold values from -0.1875 to 0.1875
- feed_gain: float32 [2048], replicated, may hold values from 0.1 to 1.9
- feed_up: bfloat16 [2048, 8192], P('sp', 'tp'), may hold values from -0.125 to 0.125
- feed_down: bfloat16 [8192, 2048], P('tp', 'sp'), may hold values from -0.0625 to 0.0625
Outputs:
- layer_out: bfloat16 [2048, 2048], P(('grp', 'sp', 'tp')), parts along dimension 0
There are 2 independent parts, one for each index of `grp`. A program takes and returns all parts, laid end to end along the dimension named above; an argument that names none is the same for every part. Nothing has to cross between parts.
All inputs are finite; a program needn't handle non-finite values.
Results may differ from a plain program's by a relative error of at most 0.02.
Values may be sent and summed in bfloat16 or wider, within the bound.
A program may use at most 128 MiB of HBM per device.

v0:
```python
import math
import jax
import jax.numpy as jnp
from jax import lax
from jax.sharding import PartitionSpec as P

QUERY_KEY_PLAIN = 64
QUERY_KEY_ROTARY = 32
VALUE_HEAD_SIZE = 64


def normalize(values, gain):
    floats = values.astype(jnp.float32)
    return floats * lax.rsqrt(jnp.mean(floats * floats, axis=-1, keepdims=True) + 1e-06) * gain


def rotate(values, position):
    half_size = values.shape[-1] // 2
    inverse = 10000.0 ** (-jnp.arange(half_size, dtype=jnp.float32) * 2.0 / values.shape[-1])
    angles = position[:, None] * inverse[None, :]
    cosine = jnp.concatenate([jnp.cos(angles), jnp.cos(angles)], axis=-1)
    sine = jnp.concatenate([jnp.sin(angles), jnp.sin(angles)], axis=-1)
    shape = (values.shape[0],) + (1,) * (values.ndim - 2) + (values.shape[-1],)
    turned = jnp.concatenate([-values[..., half_size:], values[..., :half_size]], axis=-1)
    return values * cosine.reshape(shape) + turned * sine.reshape(shape)


def on_device(
    hidden_in,
    query_latent_rows,
    key_value_latent,
    rotary_key,
    query_norm_gain,
    key_value_gain,
    query_up_weight,
    key_value_up_weight,
    out_proj,
    feed_gain,
    feed_up,
    feed_down,
):
    tokens_here = hidden_in.shape[0]
    heads_here = query_up_weight.shape[1] // (QUERY_KEY_PLAIN + QUERY_KEY_ROTARY)
    position = (lax.axis_index("sp") * tokens_here + jnp.arange(tokens_here)).astype(jnp.float32)
    scale_factor = (QUERY_KEY_PLAIN + QUERY_KEY_ROTARY) ** (-0.5)
    query_norm = normalize(query_latent_rows, query_norm_gain).astype(jnp.bfloat16)
    queries = jnp.dot(query_norm, query_up_weight, preferred_element_type=jnp.float32).reshape(
        tokens_here, heads_here, QUERY_KEY_PLAIN + QUERY_KEY_ROTARY
    )
    queries = jnp.concatenate(
        [queries[..., :QUERY_KEY_PLAIN], rotate(queries[..., QUERY_KEY_PLAIN:], position)], axis=-1
    ).astype(jnp.bfloat16)
    query_plain = queries[..., :QUERY_KEY_PLAIN]
    query_turned = queries[..., QUERY_KEY_PLAIN:]
    latent = normalize(key_value_latent, key_value_gain).astype(jnp.bfloat16)
    key_rope = rotate(rotary_key.astype(jnp.float32), position).astype(jnp.bfloat16)

    def attend_block(carry, key_plain, value_rows, rope_rows):
        row_max, denom, accum = carry
        scores = jnp.einsum(
            "qhd,khd->hqk", query_plain, key_plain, preferred_element_type=jnp.float32
        )
        scores = scores + jnp.einsum(
            "qhd,kd->hqk", query_turned, rope_rows, preferred_element_type=jnp.float32
        )
        scores = scores * scale_factor
        new_max = jnp.maximum(row_max, jnp.max(scores, axis=-1))
        expo = jnp.exp(scores - new_max[:, :, None])
        factor = jnp.exp(row_max - new_max)
        denom = denom * factor + jnp.sum(expo, axis=-1)
        update = jnp.einsum(
            "hqk,khd->qhd",
            expo.astype(jnp.bfloat16),
            value_rows,
            preferred_element_type=jnp.float32,
        )
        accum = accum * jnp.transpose(factor)[:, :, None] + update
        return (new_max, denom, accum)

    start_carry = (
        jnp.full((heads_here, tokens_here), -1e30, jnp.float32),
        jnp.zeros((heads_here, tokens_here), jnp.float32),
        jnp.zeros((tokens_here, heads_here, VALUE_HEAD_SIZE), jnp.float32),
    )
    own_keys = jnp.dot(latent, key_value_up_weight, preferred_element_type=jnp.float32).astype(
        jnp.bfloat16
    )
    pieces = (
        lax.all_gather(own_keys, "sp", axis=0, tiled=True),
        lax.all_gather(key_rope, "sp", axis=0, tiled=True),
    )
    rows_in = pieces[0].shape[0]
    block = math.gcd(rows_in, 1024)

    def step_block(index, inner):
        first = index * block
        bulk = lax.dynamic_slice_in_dim(pieces[0], first, block, 0)
        rope_rows = lax.dynamic_slice_in_dim(pieces[1], first, block, 0)
        bulk = bulk.reshape(block, heads_here, QUERY_KEY_PLAIN + VALUE_HEAD_SIZE)
        return attend_block(
            inner, bulk[..., :QUERY_KEY_PLAIN], bulk[..., QUERY_KEY_PLAIN:], rope_rows
        )

    final_carry = lax.fori_loop(0, rows_in // block, step_block, start_carry)
    denom = final_carry[1]
    accum = final_carry[2]
    mixed = (
        (accum / jnp.transpose(denom)[:, :, None])
        .astype(jnp.bfloat16)
        .reshape(tokens_here, heads_here * VALUE_HEAD_SIZE)
    )
    share = tokens_here // lax.axis_size("tp")
    lead = lax.axis_index("tp") * share
    branch = lax.psum(
        jnp.dot(mixed, out_proj, preferred_element_type=jnp.float32).astype(jnp.bfloat16), "tp"
    ).astype(jnp.float32)
    middle = (hidden_in.astype(jnp.float32) + branch).astype(jnp.bfloat16)
    normed = normalize(middle, feed_gain).astype(jnp.bfloat16)
    middle_own = lax.dynamic_slice_in_dim(middle, lead, share, 0)
    upward = jnp.dot(
        normed,
        lax.all_gather(feed_up, "sp", axis=0, tiled=True),
        preferred_element_type=jnp.float32,
    )
    activated = jnp.square(jax.nn.relu(upward)).astype(jnp.bfloat16)
    partial_sum = jnp.dot(
        activated,
        lax.all_gather(feed_down, "sp", axis=1, tiled=True),
        preferred_element_type=jnp.float32,
    )
    feed = lax.psum_scatter(
        partial_sum.astype(jnp.bfloat16), "tp", scatter_dimension=0, tiled=True
    ).astype(jnp.float32)
    return (middle_own.astype(jnp.float32) + feed).astype(jnp.bfloat16)


def solution(mesh):
    return jax.shard_map(
        on_device,
        mesh=mesh,
        in_specs=(
            P(("grp", "sp"), None),
            P(("grp", "sp"), None),
            P(("grp", "sp"), None),
            P(("grp", "sp"), None),
            P(),
            P(),
            P(None, "tp"),
            P(None, "tp"),
            P("tp", None),
            P(),
            P("sp", "tp"),
            P("tp", "sp"),
        ),
        out_specs=P(("grp", "sp", "tp"), None),
        check_vma=False,
    )
```

profile of v0, /device:TPU:0, one launch (start us, length us, event | category | flops | bytes accessed | tf_op | source)
XLA Modules:
  0.0 427.3 jit_solution(10657204658215220777)
XLA Ops:
  6.5 0.0 copy-start
  6.5 0.0 all-gather.4.cloned.1.call-start
  6.5 1.2 fusion.31
  7.7 2.2 convolution_convert_fusion.2
  9.9 0.0 all-gather.4.cloned.1.call-update
  9.9 0.0 all-reduce.2.cloned.1.call-start
  10.0 0.7 convert_element_type.75
  10.7 0.7 slice.45
  11.4 0.1 multiply_cosine_fusion
  11.6 0.7 pad_maximum_fusion
  12.3 15.3 %all_gather.13 = bf16[1024,32]{0,1:T(8,128)(2,1)S(1)} all-gather(bf16[256,32]{0,1:T(8,128)(2,1)S(1)} %get-tuple-element.26), channel_id=1, replica_groups=mesh['grp'=2,'sp'=4,'tp'=4] {'sp'}, dimensions={0}, use_global_device_ids=true | all-gather | bytes 81920 | tf_op jit(solution)/shard_map/all_gather | solution.py:90
  27.6 1.2 fusion.26
  28.8 1.6 fusion.37
  30.4 11.1 %all-gather.4.cloned.1.call-done = bf16[1024,512]{1,0:T(8,128)(2,1)} async-done(((bf16[256,512]{1,0:T(8,128)(2,1)}), bf16[1024,512]{1,0:T(8,128)(2,1)}) %all-gather.4.cloned.1.call-update) | async-done | bytes 1048592 | tf_op jit(solution)/shard_map/all_gather | solution.py:89
  41.5 1.5 copy.26
  43.0 0.7 fusion.35
  43.7 0.9 fusion.54
  44.6 1.1 fusion.1
  45.7 0.9 fusion.20
  46.5 0.0 copy-start.1
  46.6 0.0 copy-done
  46.6 1.5 convolution_convert_fusion
  48.0 0.0 copy-start.2
  48.0 0.0 all-reduce.2.cloned.1.call-update
  48.1 0.0 all-gather.6.cloned.1.call-start
  48.1 0.7 all-gather.6.cloned.1.call-update
  48.8 0.0 all-gather.8.cloned.1.call-start
  48.9 0.5 all-gather.8.cloned.1.call-update
  49.4 0.0 reduce-scatter.2.cloned.1.call-start
  49.4 34.2 %all-reduce.2.cloned.1.call-done = bf16[256,2048]{1,0:T(8,128)(2,1)} async-done(((bf16[256,2048]{1,0:T(8,128)(2,1)}), bf16[256,2048]{1,0:T(8,128)(2,1)}) %all-reduce.2.cloned.1.call-update) | async-done | bytes 1048592 | tf_op jit(solution)/shard_map/psum | solution.py:114
  83.6 0.0 copy-done.1
  83.6 1.7 fusion.5
  85.4 150.0 %all-gather.6.cloned.1.call-done = bf16[2048,2048]{1,0:T(8,128)(2,1)} async-done(((bf16[512,2048]{1,0:T(8,128)(2,1)}), bf16[2048,2048]{1,0:T(8,128)(2,1)}) %all-gather.6.cloned.1.call-update) | async-done | bytes 8388624 | tf_op jit(solution)/shard_map/all_gather | solution.py:122
  235.3 149.3 %all-gather.8.cloned.1.call-done = bf16[2048,2048]{1,0:T(8,128)(2,1)} async-done(((bf16[2048,512]{1,0:T(8,128)(2,1)}), bf16[2048,2048]{1,0:T(8,128)(2,1)}) %all-gather.8.cloned.1.call-update) | async-done | bytes 8388624 | tf_op jit(solution)/shard_map/all_gather | solution.py:128
  384.6 0.0 copy-done.2
  384.6 11.3 %convolution_convert_fusion.1 = bf16[256,2048]{1,0:T(8,128)(2,1)} fusion(bf16[2048,2048]{1,0:T(8,128)(2,1)} %all-gather.8.cloned.1.call-done, bf16[2048,2048]{1,0:T(8,128)(2,1)} %all-gather.6.cloned.1.call-done, bf16[256,2048]{1,0:T(8,128)(2,1)S(1)} %get-tuple-element.22, f32[2048]{0:T(1024)S(1)} %copy-done.2, f32[256]{0:T(256)S(1)} %add_rsqrt_fusion), kind=kOutput, calls=%fused_computation.11 | convolution fusion | flops 4299161600 | bytes 18883584 | tf_op jit(solution)/shard_map/dot_general | solution.py:126
  395.9 0.0 reduce-scatter.2.cloned.1.call-update
  395.9 23.1 %reduce-scatter.2.cloned.1.call-done = bf16[64,2048]{1,0:T(8,128)(2,1)} async-done(((bf16[256,2048]{1,0:T(8,128)(2,1)}), bf16[64,2048]{1,0:T(8,128)(2,1)}) %reduce-scatter.2.cloned.1.call-update) | async-done | bytes 262160 | tf_op jit(solution)/shard_map/reduce_scatter | solution.py:131
  419.0 1.7 add_convert_fusion.1
  (8 shorter events, 0.1 us)
Async XLA Ops:
  6.5 40.0 %copy-start = (bf16[256,2048]{1,0:T(8,128)(2,1)S(1)}, bf16[256,2048]{1,0:T(8,128)(2,1)}, u32[]{:S(2)}) copy-start(bf16[256,2048]{1,0:T(8,128)(2,1)} %param.20) | copy-start | bytes 3145732
  6.5 34.9 %all-gather.4.cloned.1.call-start = ((), (), s32[]{:S(2)}) async-start(), calls=%async_computation.1 | async-start | bytes 1310720 | tf_op jit(solution)/shard_map/all_gather | solution.py:89
  9.9 73.7 %all-reduce.2.cloned.1.call-start = ((), (), s32[]{:S(2)}) async-start(), calls=%async_computation.2 | async-start | bytes 2097152 | tf_op jit(solution)/shard_map/psum | solution.py:114
  46.5 37.1 %copy-start.1 = (bf16[256,2048]{1,0:T(8,128)(2,1)S(1)}, bf16[256,2048]{1,0:T(8,128)(2,1)}, u32[]{:S(2)}) copy-start(bf16[256,2048]{1,0:T(8,128)(2,1)} %param.12) | copy-start | bytes 3145732
  48.0 336.6 %copy-start.2 = (f32[2048]{0:T(1024)S(1)}, f32[2048]{0:T(1024)}, u32[]{:S(2)}) copy-start(f32[2048]{0:T(1024)} %param.21) | copy-start | bytes 24580
  48.1 187.3 %all-gather.6.cloned.1.call-start = ((), (), s32[]{:S(2)}) async-start(), calls=%async_computation.3 | async-start | bytes 10485760 | tf_op jit(solution)/shard_map/all_gather | solution.py:122
  48.8 335.8 %all-gather.8.cloned.1.call-start = ((), (), s32[]{:S(2)}) async-start(), calls=%async_computation.4 | async-start | bytes 10485760 | tf_op jit(solution)/shard_map/all_gather | solution.py:128
  49.4 369.6 %reduce-scatter.2.cloned.1.call-start = ((), (), s32[]{:S(2)}) async-start(), calls=%async_computation.5 | async-start | bytes 1310720 | tf_op jit(solution)/shard_map/reduce_scatter | solution.py:131
Sparse Core Ops, SparseCore 0:
  10.1 31.3 all-gather.3
  48.2 35.4 all-reduce.1
  85.2 150.0 all-gather.5
  236.8 147.7 all-gather.7
  396.0 22.9 reduce-scatter.1
where the time goes:
time: 428 us; the launch traced here: 427 us
  waiting for transfers between devices  369 us (86%)
  matrix products  19.1 us (4%)
  blocking collectives  15.3 us (4%)
  between operations  13.2 us (3%)
  other arithmetic  8.5 us (2%)
    all_gather x1, waiting for transfers between devices, on_device(): lax.all_gather(feed_up, 'sp', axis=0, tiled=True)  150 us
    all_gather x1, waiting for transfers between devices, on_device(): lax.all_gather(feed_down, 'sp', axis=1, tiled=True)  149 us
    psum x1, waiting for transfers between devices, on_device(): lax.psum(jnp.dot(mixed, out_proj, preferred_element_type=jnp.float32).ast...  34.2 us
    reduce_scatter x1, waiting for transfers between devices, on_device(): lax.psum_scatter(partial_sum.astype(jnp.bfloat16), 'tp', scatter_dimensio...  23.1 us
    all_gather x1, blocking collectives, on_device(): lax.all_gather(key_rope, 'sp', axis=0, tiled=True)  15.3 us
    dot_general x1, matrix products, on_device(): jnp.dot(activated, lax.all_gather(feed_down, 'sp', axis=1, tiled=True), p...  11.3 us
    all_gather x1, waiting for transfers between devices, on_device(): lax.all_gather(own_keys, 'sp', axis=0, tiled=True)  11.1 us
  transfers between devices with their start and end apart: 5, of which 5 were waited for; matrix products, arithmetic and copies ran while one was open for 2% of the time, Pallas kernels for 0%

commit v1 on v0

--- a/solution.py
+++ b/solution.py
@@ -111,8 +111,11 @@
     )
     share = tokens_here // lax.axis_size("tp")
     lead = lax.axis_index("tp") * share
-    branch = lax.psum(
-        jnp.dot(mixed, out_proj, preferred_element_type=jnp.float32).astype(jnp.bfloat16), "tp"
+    branch = jnp.sum(
+        lax.all_gather(
+            jnp.dot(mixed, out_proj, preferred_element_type=jnp.float32).astype(jnp.bfloat16), "tp"
+        ),
+        axis=0,
     ).astype(jnp.float32)
     middle = (hidden_in.astype(jnp.float32) + branch).astype(jnp.bfloat16)
     normed = normalize(middle, feed_gain).astype(jnp.bfloat16)

time: 428 us -> 425 us (level)
  waiting for transfers between devices: 369 us -> 363 us
    psum x1 -> x0, waiting for transfers between devices: 34.2 us -> none  [on_device(): lax.psum(jnp.dot(mixed, out_proj, preferred_element_type=jnp.float32).ast...]
    all_gather x0 -> x1, waiting for transfers between devices: none -> 32.4 us  [on_device(): lax.all_gather(jnp.dot(mixed, out_proj, preferred_element_type=jnp.float3...]
where the time goes in v1:
time: 425 us
  waiting for transfers between devices  363 us (85%)
  matrix products  19 us (4%)
  blocking collectives  15.4 us (4%)
  between operations  13.2 us (3%)
  other arithmetic  11.6 us (3%)
    all_gather x1, waiting for transfers between devices, on_device(): lax.all_gather(feed_up, 'sp', axis=0, tiled=True)  149 us
    all_gather x1, waiting for transfers between devices, on_device(): lax.all_gather(feed_down, 'sp', axis=1, tiled=True)  146 us
    all_gather x1, waiting for transfers between devices, on_device(): lax.all_gather(jnp.dot(mixed, out_proj, preferred_element_type=jnp.float3...  32.4 us
    reduce_scatter x1, waiting for transfers between devices, on_device(): lax.psum_scatter(partial_sum.astype(jnp.bfloat16), 'tp', scatter_dimensio...  23.1 us
    all_gather x1, blocking collectives, on_device(): lax.all_gather(key_rope, 'sp', axis=0, tiled=True)  15.4 us
    dot_general x1, matrix products, on_device(): jnp.dot(activated, lax.all_gather(feed_down, 'sp', axis=1, tiled=True), p...  11.3 us
    all_gather x1, waiting for transfers between devices, on_device(): lax.all_gather(own_keys, 'sp', axis=0, tiled=True)  11 us
  transfers between devices with their start and end apart: 5, of which 5 were waited for; matrix products, arithmetic and copies ran while one was open for 2% of the time, Pallas kernels for 0%

profile of v1, /device:TPU:0, one launch (start us, length us, event | category | flops | bytes accessed | tf_op | source)
XLA Modules:
  0.0 424.9 jit_solution(8367574819751764297)
XLA Ops:
  6.5 0.0 copy-start
  6.5 0.0 all-gather.6.cloned.1.call-start
  6.5 1.2 fusion.31
  7.7 2.2 convolution_convert_fusion.2
  9.9 0.0 all-gather.6.cloned.1.call-update
  9.9 0.0 all-gather.12.cloned.1.call-start
  10.0 0.7 convert_element_type.77
  10.7 0.7 slice.45
  11.4 0.1 multiply_cosine_fusion
  11.6 0.7 pad_maximum_fusion
  12.3 15.4 %all_gather.19 = bf16[1024,32]{0,1:T(8,128)(2,1)S(1)} all-gather(bf16[256,32]{0,1:T(8,128)(2,1)S(1)} %get-tuple-element.26), channel_id=1, replica_groups=mesh['grp'=2,'sp'=4,'tp'=4] {'sp'}, dimensions={0}, use_global_device_ids=true | all-gather | bytes 81920 | tf_op jit(solution)/shard_map/all_gather | solution.py:90
  27.7 1.2 fusion.26
  28.8 1.6 fusion.37
  30.5 11.0 %all-gather.6.cloned.1.call-done = bf16[1024,512]{1,0:T(8,128)(2,1)} async-done(((bf16[256,512]{1,0:T(8,128)(2,1)}), bf16[1024,512]{1,0:T(8,128)(2,1)}) %all-gather.6.cloned.1.call-update) | async-done | bytes 1048592 | tf_op jit(solution)/shard_map/all_gather | solution.py:89
  41.5 1.5 copy.26
  43.0 0.7 fusion.35
  43.7 0.9 fusion.54
  44.6 1.1 fusion.1
  45.7 0.9 fusion.20
  46.5 0.0 copy-done
  46.5 1.4 convolution_convert_fusion
  48.0 0.0 all-gather.12.cloned.1.call-update
  48.0 0.0 all-gather.10.cloned.1.call-start
  48.1 0.7 all-gather.10.cloned.1.call-update
  48.8 0.0 all-gather.8.cloned.1.call-start
  48.8 0.5 all-gather.8.cloned.1.call-update
  49.3 0.0 reduce-scatter.2.cloned.1.call-start
  49.4 32.4 %all-gather.12.cloned.1.call-done = bf16[1024,2048]{1,0:T(8,128)(2,1)} async-done(((bf16[256,2048]{1,0:T(8,128)(2,1)}), bf16[1024,2048]{1,0:T(8,128)(2,1)}) %all-gather.12.cloned.1.call-update) | async-done | bytes 4194320 | tf_op jit(solution)/shard_map/all_gather | solution.py:115
  81.7 0.0 copy-start.1
  81.8 3.1 reduce_sum.55
  84.8 1.7 fusion.5
  86.6 146.4 %all-gather.10.cloned.1.call-done = bf16[2048,2048]{1,0:T(8,128)(2,1)} async-done(((bf16[2048,512]{1,0:T(8,128)(2,1)}), bf16[2048,2048]{1,0:T(8,128)(2,1)}) %all-gather.10.cloned.1.call-update) | async-done | bytes 8388624 | tf_op jit(solution)/shard_map/all_gather | solution.py:131
  233.0 149.3 %all-gather.8.cloned.1.call-done = bf16[2048,2048]{1,0:T(8,128)(2,1)} async-done(((bf16[512,2048]{1,0:T(8,128)(2,1)}), bf16[2048,2048]{1,0:T(8,128)(2,1)}) %all-gather.8.cloned.1.call-update) | async-done | bytes 8388624 | tf_op jit(solution)/shard_map/all_gather | solution.py:125
  382.2 0.0 copy-done.1
  382.2 11.3 %convolution_convert_fusion.1 = bf16[256,2048]{1,0:T(8,128)(2,1)} fusion(bf16[2048,2048]{1,0:T(8,128)(2,1)} %all-gather.10.cloned.1.call-done, bf16[2048,2048]{1,0:T(8,128)(2,1)} %all-gather.8.cloned.1.call-done, bf16[256,2048]{1,0:T(8,128)(2,1)S(1)} %get-tuple-element.22, f32[2048]{0:T(1024)S(1)} %copy-done.1, f32[256]{0:T(256)S(1)} %add_rsqrt_fusion), kind=kOutput, calls=%fused_computation.11 | convolution fusion | flops 4299161600 | bytes 18883584 | tf_op jit(solution)/shard_map/dot_general | solution.py:129
  393.5 0.0 reduce-scatter.2.cloned.1.call-update
  393.5 23.1 %reduce-scatter.2.cloned.1.call-done = bf16[64,2048]{1,0:T(8,128)(2,1)} async-done(((bf16[256,2048]{1,0:T(8,128)(2,1)}), bf16[64,2048]{1,0:T(8,128)(2,1)}) %reduce-scatter.2.cloned.1.call-update) | async-done | bytes 262160 | tf_op jit(solution)/shard_map/reduce_scatter | solution.py:134
  416.7 1.7 add_convert_fusion.1
  (8 shorter events, 0.1 us)
Async XLA Ops:
  6.5 40.0 %copy-start = (bf16[256,2048]{1,0:T(8,128)(2,1)S(1)}, bf16[256,2048]{1,0:T(8,128)(2,1)}, u32[]{:S(2)}) copy-start(bf16[256,2048]{1,0:T(8,128)(2,1)} %param.20) | copy-start | bytes 3145732
  6.5 34.9 %all-gather.6.cloned.1.call-start = ((), (), s32[]{:S(2)}) async-start(), calls=%async_computation.1 | async-start | bytes 1310720 | tf_op jit(solution)/shard_map/all_gather | solution.py:89
  9.9 71.8 %all-gather.12.cloned.1.call-start = ((), (), s32[]{:S(2)}) async-start(), calls=%async_computation.5 | async-start | bytes 5242880 | tf_op jit(solution)/shard_map/all_gather | solution.py:115
  48.0 185.0 %all-gather.10.cloned.1.call-start = ((), (), s32[]{:S(2)}) async-start(), calls=%async_computation.3 | async-start | bytes 10485760 | tf_op jit(solution)/shard_map/all_gather | solution.py:131
  48.8 333.5 %all-gather.8.cloned.1.call-start = ((), (), s32[]{:S(2)}) async-start(), calls=%async_computation.2 | async-start | bytes 10485760 | tf_op jit(solution)/shard_map/all_gather | solution.py:125
  49.3 367.3 %reduce-scatter.2.cloned.1.call-start = ((), (), s32[]{:S(2)}) async-start(), calls=%async_computation.4 | async-start | bytes 1310720 | tf_op jit(solution)/shard_map/reduce_scatter | solution.py:134
  81.7 300.5 %copy-start.1 = (f32[2048]{0:T(1024)S(1)}, f32[2048]{0:T(1024)}, u32[]{:S(2)}) copy-start(f32[2048]{0:T(1024)} %param.21) | copy-start | bytes 24580
Sparse Core Ops, SparseCore 0:
  10.1 31.3 all-gather.5
  48.1 33.5 all-gather.11
  83.3 149.6 all-gather.9
  234.4 147.7 all-gather.7
  393.7 22.9 reduce-scatter.1
